TPU v7x, 32 devices: a whole 2x2x4 slice. The times are simulated.
32 devices in a mesh: kv: 16 (over z, y, x), tp: 2 (over core).
Axes of the slice: x: 2, y: 2, z: 4, core: 2. Of those that a mesh axis runs over, the one named last changes fastest.
Arguments:
- tokens: bfloat16 [4, 4, 4096], replicated, may hold values from -6 to 6
- parents: int32 [4, 4], replicated, may hold values from -1 to 2, as said below
- lengths: int32 [4], replicated, may hold values from 1 to 2040, as said below
- accepted: int32 [4], replicated, may hold values from 0 to 4
- in_gain: float32 [4096], replicated, may hold values from 0.1 to 1.9
- w_query: bfloat16 [4096, 3072], P('kv', 'tp'), may hold values from -0.09375 to 0.09375
- w_latent: bfloat16 [4096, 1024], P('kv'), may hold values from -0.09375 to 0.09375
- w_rope_key: bfloat16 [4096, 32], replicated, may hold values from -0.09375 to 0.09375
- latent_gain: float32 [1024], replicated, may hold values from 0.1 to 1.9
- query_gain: float32 [96], replicated, may hold values from 0.4 to 160, as said below
- key_gain: float32 [96], replicated, may hold values from 0.1 to 1.9
- w_key_up: bfloat16 [1024, 2048], P(None, 'tp'), may hold values from -0.1875 to 0.1875
- w_value_up: bfloat16 [1024, 2048], P(None, 'tp'), may hold values from -0.1875 to 0.1875
- w_out: bfloat16 [2048, 4096], P('tp', 'kv'), may hold values from -1 to 1
- out_gain: float32 [4096], P('kv'), may hold values from 0.1 to 1.9
- cache_latent: bfloat16 [4, 2048, 1024], P(None, 'kv'), may hold values from -6 to 6
- cache_rope: bfloat16 [4, 2048, 32], P(None, 'kv'), may hold values from -6 to 6
Outputs:
- mixed: bfloat16 [4, 4, 4096], P(None, None, 'kv')
- new_latent: bfloat16 [4, 2048, 1024], P(None, 'kv')
- new_rope: bfloat16 [4, 2048, 32], P(None, 'kv')
Inputs may be any that keep to these rules, and one draw needn't show every extreme that they name: parents[s, 0] is -1; for i of 1 or more parents[s, i] lies in 0 to i - 1. `lengths`: the first sequence's length is at most 8, the last one's at least 1912. `query_gain`: positive.
All inputs are finite; a program needn't handle non-finite values.
Results may differ from a plain program's by a relative error of at most 0.008.
The roundings to bfloat16 on the way count: a program that leaves them out, or rounds other values in their place, can miss the bound.
Values sent between devices are 32-bit elements; how exact they have to be, the bound alone decides.
A program may use at most 64 MiB of HBM per device.

v0:
```python
import jax
import jax.numpy as jnp
from jax import lax
from jax.sharding import PartitionSpec as P

D = 4096
NOPE = 64
ROPE = 32
QK = 96
VDIM = 64


epsilon = 1e-06
rope_base = 10000.0


def combined_all(value, axis, join):
    pieces = jax.tree.map(lambda part: lax.all_gather(part, axis), value)
    head = jax.tree.map(lambda part: part[0], pieces)
    tail = jax.tree.map(lambda part: part[1:], pieces)
    running, _ = lax.scan(lambda running, piece: (join(running, piece), None), head, tail)
    return running


def ancestry(parents):
    prop_count = parents.shape[-1]
    indices = jnp.arange(prop_count, dtype=jnp.int32)
    step_map = (parents[..., :, None] == indices).astype(jnp.int32)
    identity_map = jnp.broadcast_to(
        (indices[:, None] == indices[None, :]).astype(jnp.int32), step_map.shape
    )
    reached = identity_map
    hop_map = identity_map
    for step_index in range(prop_count - 1):
        hop_map = jnp.einsum("sij,sjk->sik", hop_map, step_map)
        reached = reached + hop_map
    return reached


def angles(positions):
    halfway = ROPE // 2
    inverse = rope_base ** (-jnp.arange(halfway, dtype=jnp.float32) / halfway)
    angle = positions.astype(jnp.float32)[..., None] * inverse
    return (jnp.cos(angle), jnp.sin(angle))


def rotate(vectors, cosine, sine_part):
    halfway = vectors.shape[-1] // 2
    leading = vectors[..., :halfway]
    trailing = vectors[..., halfway:]
    return jnp.concatenate(
        [leading * cosine - trailing * sine_part, trailing * cosine + leading * sine_part], -1
    )


def split_keys(latents, rope_rows, w_key_up, key_gain):
    head_count = w_key_up.shape[1] // NOPE
    nope = jnp.dot(latents, w_key_up, preferred_element_type=jnp.float32)
    nope = nope.reshape(latents.shape[:2] + (head_count, NOPE))
    rope_wide = rope_rows.astype(jnp.float32)[:, :, None, :]
    squares = jnp.sum(nope * nope, -1) + jnp.sum(rope_wide * rope_wide, -1)
    factor = lax.rsqrt(squares / QK + epsilon)[..., None]
    key_nope = (nope * factor * key_gain[:NOPE]).astype(jnp.bfloat16)
    key_rope = (rope_wide * factor * key_gain[NOPE:]).astype(jnp.bfloat16)
    return (key_nope, key_rope)


def attend_block(query, key_nope, key_rope, latents, visible):
    score_scale = QK ** (-0.5)
    scores = jnp.einsum(
        "sphd,slhd->shpl", query[..., :NOPE], key_nope, preferred_element_type=jnp.float32
    )
    scores = scores + jnp.einsum(
        "sphd,slhd->shpl", query[..., NOPE:], key_rope, preferred_element_type=jnp.float32
    )
    scores = jnp.where(visible, scores * score_scale, -1e30)
    peaks = jnp.max(scores, -1)
    weights = jnp.where(visible, jnp.exp(scores - peaks[..., None]), 0.0)
    totals = jnp.sum(weights, -1)
    summed = jnp.einsum(
        "shpl,slc->sphc", weights.astype(jnp.bfloat16), latents, preferred_element_type=jnp.float32
    )
    return (jnp.swapaxes(peaks, 1, 2), jnp.swapaxes(totals, 1, 2), summed)


def combine(left_part, right_part):
    left_peak, left_total, left_sum = left_part
    right_peak, right_total, right_sum = right_part
    highest = jnp.maximum(left_peak, right_peak)
    left_scale = jnp.exp(left_peak - highest)
    right_scale = jnp.exp(right_peak - highest)
    return (
        highest,
        left_total * left_scale + right_total * right_scale,
        left_sum * left_scale[..., None] + right_sum * right_scale[..., None],
    )


def body(
    tokens,
    parents,
    lengths,
    accepted,
    in_gain,
    w_query,
    w_latent,
    w_rope_key,
    latent_gain,
    query_gain,
    key_gain,
    w_key_up,
    w_value_up,
    w_out,
    out_gain,
    cache_latent,
    cache_rope,
):
    seq_count, prop_count, model_width = tokens.shape
    row_count = seq_count * prop_count
    head_count = w_key_up.shape[1] // NOPE
    flattened = tokens.reshape(row_count, model_width).astype(jnp.float32)
    normed = (
        flattened
        * lax.rsqrt(jnp.mean(flattened * flattened, -1, keepdims=True) + epsilon)
        * in_gain
    ).astype(jnp.bfloat16)
    part_rows = w_query.shape[0]
    normed_part = lax.dynamic_slice_in_dim(normed, lax.axis_index("kv") * part_rows, part_rows, 1)
    query_part = jnp.dot(normed_part, w_query, preferred_element_type=jnp.float32)
    latent_part = jnp.dot(normed_part, w_latent, preferred_element_type=jnp.float32)
    query_raw, latent_raw = lax.psum((query_part, latent_part), "kv")
    rope_raw = jnp.dot(normed, w_rope_key, preferred_element_type=jnp.float32).reshape(
        seq_count, prop_count, ROPE
    )
    latent_raw = latent_raw.reshape(seq_count, prop_count, -1)
    reached = ancestry(parents)
    anchor = lengths + accepted
    positions = anchor[:, None] + jnp.sum(reached, -1) - 1
    cosine, sine_part = angles(positions)
    query_raw = query_raw.reshape(seq_count, prop_count, head_count, QK)
    turned = rotate(query_raw[..., NOPE:], cosine[:, :, None, :], sine_part[:, :, None, :])
    joined = jnp.concatenate([query_raw[..., :NOPE], turned], -1)
    query = (
        joined * lax.rsqrt(jnp.mean(joined * joined, -1, keepdims=True) + epsilon) * query_gain
    ).astype(jnp.bfloat16)
    latent_new = (
        latent_raw
        * lax.rsqrt(jnp.mean(latent_raw * latent_raw, -1, keepdims=True) + epsilon)
        * latent_gain
    ).astype(jnp.bfloat16)
    rope_new = rotate(rope_raw, cosine, sine_part).astype(jnp.bfloat16)
    shard_len = cache_latent.shape[1]
    places = lax.axis_index("kv") * shard_len + jnp.arange(shard_len, dtype=jnp.int32)
    offset = places[None, :] - anchor[:, None]
    selected = offset[:, :, None] == jnp.arange(prop_count, dtype=jnp.int32)[None, None, :]
    filled = jnp.any(selected, -1)[..., None]
    selector = selected.astype(jnp.bfloat16)
    placed_latent = jnp.einsum(
        "slp,spc->slc", selector, latent_new, preferred_element_type=jnp.float32
    ).astype(jnp.bfloat16)
    placed_rope = jnp.einsum(
        "slp,spc->slc", selector, rope_new, preferred_element_type=jnp.float32
    ).astype(jnp.bfloat16)
    new_latent = jnp.where(filled, placed_latent, cache_latent)
    new_rope = jnp.where(filled, placed_rope, cache_rope)
    key_nope, key_rope = split_keys(cache_latent, cache_rope, w_key_up, key_gain)
    cache_seen = (places[None, :] < anchor[:, None])[:, None, None, :]
    block_peak, block_total, block_sum = attend_block(
        query, key_nope, key_rope, cache_latent, cache_seen
    )
    own_nope, own_rope = split_keys(latent_new, rope_new, w_key_up, key_gain)
    own_seen = (reached > 0)[:, None, :, :]
    own_peak, own_total, own_sum = attend_block(query, own_nope, own_rope, latent_new, own_seen)
    value_up = w_value_up.astype(jnp.float32).reshape(w_value_up.shape[0], head_count, VDIM)

    def to_values(summed):
        return jnp.einsum("sphc,chd->sphd", summed, value_up, precision=lax.Precision.HIGHEST)

    far_peak, far_total, far_sum = combined_all(
        (block_peak, block_total, to_values(block_sum)), "kv", combine
    )
    near_sum = to_values(own_sum)
    joint_peak, joint_total, joint_sum = combine(
        (far_peak, far_total, far_sum), (own_peak, own_total, near_sum)
    )
    attended = joint_sum / joint_total[..., None]
    values_low = attended.astype(jnp.bfloat16).reshape(row_count, head_count * VDIM)
    projected_part = jnp.dot(values_low, w_out, preferred_element_type=jnp.float32)
    projected = lax.psum(projected_part, "tp")
    squares = lax.psum(jnp.sum(projected * projected, -1), "kv")
    mixed = (projected * lax.rsqrt(squares / D + epsilon)[:, None] * out_gain).astype(jnp.bfloat16)
    return (mixed.reshape(seq_count, prop_count, -1), new_latent, new_rope)


def solution(mesh):
    return jax.shard_map(
        body,
        mesh=mesh,
        in_specs=(
            P(),
            P(),
            P(),
            P(),
            P(),
            P("kv", "tp"),
            P("kv", None),
            P(),
            P(),
            P(),
            P(),
            P(None, "tp"),
            P(None, "tp"),
            P("tp", "kv"),
            P("kv"),
            P(None, "kv", None),
            P(None, "kv", None),
        ),
        out_specs=(P(None, None, "kv"), P(None, "kv", None), P(None, "kv", None)),
        check_vma=False,
    )
```

profile of v0, /device:TPU:0, one launch (start us, length us, event | category | flops | bytes accessed | tf_op | source)
XLA Modules:
  0.0 361.5 jit_solution(694344861112431928)
XLA Ops:
  7.3 1.2 multiply_reduce_fusion.1
  8.5 0.9 reshape.252
  9.5 0.8 dynamic-slice
  10.7 0.7 copy.75
  11.4 1.9 fusion.70
  14.5 4.2 %multiply_reduce_fusion = (f32[4,128,16]{1,2,0:T(8,128)S(1)}, f32[4,128,1024]{1,2,0:T(8,128)}) fusion(bf16[4,128,1024]{2,1,0:T(8,128)(2,1)S(1)} %copy-done.1, bf16[1024,1024]{1,0:T(8,128)(2,1)} %param.30), kind=kOutput, calls=%fused_computation.13 | convolution fusion | flops 1074782208 | bytes 5275648 | tf_op jit(solution)/shard_map/dot_general | solution.py:58
  18.8 0.9 fusion.13
  19.8 4.0 %copy.88 = bf16[1024,1024]{0,1:T(8,128)(2,1)} copy(bf16[1024,1024]{1,0:T(8,128)(2,1)} %param.30) | data formatting | bytes 4194304 | tf_op args[11]
  24.0 2.9 copy.83
  27.1 97.9 %all-reduce.3.cloned.1.call-done = (f32[16,1024]{1,0:T(8,128)}, f32[4,4,16,96]{3,1,2,0:T(4,128)}) async-done(((f32[16,1024]{1,0:T(8,128)}, f32[4,4,16,96]{3,1,2,0:T(4,128)}), (f32[16,1024]{1,0:T(8,128)}, f32[4,4,16,96]{3,1,2,0:T(4,128)})) %all-reduce.3.cloned.1.call-update) | async-done | bytes 163856 | tf_op jit(solution)/shard_map/psum | solution.py:131
  125.0 1.2 multiply_subtract_fusion
  126.2 1.2 multiply_reduce_fusion.3
  127.5 1.2 multiply_convert_fusion.8
  128.7 2.1 fusion.14
  131.5 39.5 %all-gather.1 = f32[64,4,16]{2,1,0:T(4,128)S(1)} all-gather(f32[4,4,16]{2,1,0:T(4,128)S(1)} %copy.81), channel_id=3, replica_groups=mesh['kv'=16,'tp'=2] {'kv'}, dimensions={0}, use_global_device_ids=true | all-gather | bytes 17408 | tf_op jit(solution)/shard_map/all_gather | solution.py:18
  171.1 36.3 %all-gather = f32[64,4,16]{2,1,0:T(4,128)S(1)} all-gather(f32[4,4,16]{2,1,0:T(4,128)S(1)} %copy.80), channel_id=2, replica_groups=mesh['kv'=16,'tp'=2] {'kv'}, dimensions={0}, use_global_device_ids=true | all-gather | bytes 17408 | tf_op jit(solution)/shard_map/all_gather | solution.py:18
  208.8 1.2 add_rsqrt_fusion.5
  210.0 1.5 convolution_bitcast_fusion.1
  211.5 3.3 convolution_bitcast_fusion.3
  215.1 3.2 multiply_reduce_fusion.2
  218.3 0.9 fusion.31
  219.3 1.1 copy.90
  220.3 1.8 fusion.30
  222.2 1.1 copy.89
  223.5 1.4 convolution_bitcast_fusion
  224.9 2.8 fusion.6
  227.7 46.0 %all-gather.5.cloned.1.call-done = f32[64,4,16,64]{3,1,0,2:T(4,128)} async-done(((f32[4,4,16,64]{3,1,0,2:T(4,128)}), f32[64,4,16,64]{3,1,0,2:T(4,128)}) %all-gather.5.cloned.1.call-update) | async-done | bytes 1048592 | tf_op jit(solution)/shard_map/all_gather | solution.py:18
  273.7 0.9 slice.80
  274.7 3.0 slice.83
  277.7 27.5 %while.14 = (s32[]{:T(128)}, f32[4,4,16]{2,1,0:T(4,128)S(1)}, f32[4,4,16]{2,1,0:T(4,128)S(1)}, f32[4,4,16,64]{3,2,1,0:T(8,128)S(1)}, f32[15,4,4,16]{3,2,1,0:T(4,...) while((s32[]{:T(128)}, f32[4,4,16]{2,1,0:T(4,128)S(1)}, ...), condition=%wide.region_9.10_spmd, body=%wide.region_8.9_spmd.sunk | while | flops 50690 | bytes 338013 | solution.py:21
  277.7 0.7 fusion.91
  278.4 0.9 constant_dynamic-slice_fusion.2
  279.5 0.7 fusion.91
  280.2 0.9 constant_dynamic-slice_fusion.2
  281.3 0.7 fusion.91
  282.1 0.9 constant_dynamic-slice_fusion.2
  283.2 0.7 fusion.91
  283.9 0.9 constant_dynamic-slice_fusion.2
  285.0 0.7 fusion.91
  285.7 0.9 constant_dynamic-slice_fusion.2
  286.8 0.7 fusion.91
  287.6 0.9 constant_dynamic-slice_fusion.2
  288.7 0.7 fusion.91
  289.4 0.9 constant_dynamic-slice_fusion.2
  290.5 0.7 fusion.91
  291.2 0.9 constant_dynamic-slice_fusion.2
  292.3 0.7 fusion.91
  293.1 0.9 constant_dynamic-slice_fusion.2
  294.2 0.7 fusion.91
  294.9 0.9 constant_dynamic-slice_fusion.2
  296.0 0.7 fusion.91
  296.7 0.9 constant_dynamic-slice_fusion.2
  297.8 0.7 fusion.91
  298.6 0.9 constant_dynamic-slice_fusion.2
  299.7 0.7 fusion.91
  300.4 0.9 constant_dynamic-slice_fusion.2
  301.5 0.7 fusion.91
  302.2 0.9 constant_dynamic-slice_fusion.2
  303.3 0.7 fusion.91
  304.1 0.9 constant_dynamic-slice_fusion.2
  306.6 0.7 copy.97
  307.3 3.9 %fusion.12 = bf16[4,4,16,64]{3,1,0,2:T(4,128)(2,1)S(1)} fusion(bf16[1024,16,64,1]{0,2,3,1:T(8,128)(2,1)S(1)} %bitcast.103, f32[4,4,16,1024]{3,2,1,0:T(8,128)} %convolution_bitcast_fusion, f32[4,4,16,64]{3,2,1,0:T(8,128)S(1)} %get-tuple-element.42, f32[4,4,16]{1,0,2:T(4,128)} %copy.100, f32[4,4,16]{1,0,2:T(4,128)} %copy.97, f32[4,4,16]{1,0,2:T(4,128)} %copy.93), kind=kOutput, calls=%fused_computation.26 | convolution fusion | flops 201408512 | bytes 3247104 | tf_op jit(solution)/shard_map/sphc,chd->sphd/dot_general | solution.py:177
  311.5 3.4 psum.30
  315.0 38.9 %psum.31 = f32[16]{0:T(128)S(1)} all-reduce(f32[16]{0:T(128)S(1)} %multiply_reduce_fusion.6), channel_id=1, replica_groups=mesh['kv'=16,'tp'=2] {'kv'}, use_global_device_ids=true, to_apply=%region_18.19 | all-reduce | flops 16 | bytes 128 | tf_op jit(solution)/shard_map/psum | solution.py:190
  (116 shorter events, 10.0 us)
Async XLA Ops:
  7.2 3.1 copy-start
  7.2 6.7 %copy-start.3 = (bf16[4,4,4096]{2,1,0:T(4,128)(2,1)S(1)}, bf16[4,4,4096]{2,1,0:T(4,128)(2,1)}, u32[]{:S(2)}) copy-start(bf16[4,4,4096]{2,1,0:T(4,128)(2,1)} %param.19) | copy-start | bytes 393220
  7.2 6.7 %copy-start.15 = (f32[4096]{0:T(1024)S(1)}, f32[4096]{0:T(1024)}, u32[]{:S(2)}) copy-start(f32[4096]{0:T(1024)} %param.23) | copy-start | bytes 49156
  7.2 6.2 %copy-start.9 = (s32[4,4]{1,0:T(4,128)S(1)}, s32[4,4]{1,0:T(4,128)}, u32[]{:S(2)}) copy-start(s32[4,4]{1,0:T(4,128)} %param.20) | copy-start | bytes 196
  7.2 6.6 %copy-start.16 = (bf16[4096,32]{0,1:T(8,128)(2,1)S(1)}, bf16[4096,32]{0,1:T(8,128)(2,1)}, u32[]{:S(2)}) copy-start(bf16[4096,32]{0,1:T(8,128)(2,1)} %param.26) | copy-start | bytes 786436
  7.2 7.0 %copy-start.7 = (bf16[4,128,32]{1,2,0:T(8,128)(2,1)S(1)}, bf16[4,128,32]{1,2,0:T(8,128)(2,1)}, u32[]{:S(2)}) copy-start(bf16[4,128,32]{1,2,0:T(8,128)(2,1)} %param.35) | copy-start | bytes 98308
  7.2 7.0 %copy-start.17 = (s32[4]{0:T(128)S(1)}, s32[4]{0:T(128)}, u32[]{:S(2)}) copy-start(s32[4]{0:T(128)} %param.21) | copy-start | bytes 52
  7.2 7.0 %copy-start.18 = (s32[4]{0:T(128)S(1)}, s32[4]{0:T(128)}, u32[]{:S(2)}) copy-start(s32[4]{0:T(128)} %param.22) | copy-start | bytes 52
  7.3 7.2 %copy-start.1 = (bf16[4,128,1024]{2,1,0:T(8,128)(2,1)S(1)}, bf16[4,128,1024]{2,1,0:T(8,128)(2,1)}, u32[]{:S(2)}) copy-start(bf16[4,128,1024]{2,1,0:T(8,128)(2,1)} %param.34) | copy-start | bytes 3145732
  7.3 117.8 %all-reduce.3.cloned.1.call-start = ((), (), s32[]{:S(2)}) async-start(), calls=%async_computation.1 | async-start | bytes 393216 | tf_op jit(solution)/shard_map/psum | solution.py:131
  13.3 260.4 %all-gather.5.cloned.1.call-start = ((), (), s32[]{:S(2)}) async-start(), calls=%async_computation | async-start | bytes 2228224 | tf_op jit(solution)/shard_map/all_gather | solution.py:18
  19.8 4.0 %copy-start.13 = (f32[96]{0:T(128)S(1)}, f32[96]{0:T(128)}, u32[]{:S(2)}) copy-start(f32[96]{0:T(128)} %param.29) | copy-start | bytes 1156
  23.8 106.9 %copy-start.19 = (f32[32]{0:T(128)}, f32[32]{0:T(128)S(1)}, u32[]{:S(2)}) copy-start(f32[32]{0:T(128)S(1)} %slice.58) | copy-start | bytes 388
  24.0 103.5 %copy-start.12 = (f32[96]{0:T(128)S(1)}, f32[96]{0:T(128)}, u32[]{:S(2)}) copy-start(f32[96]{0:T(128)} %param.28) | copy-start | bytes 1156
  128.7 79.5 %copy-start.2 = (f32[16,1024]{1,0:T(8,128)S(1)}, f32[16,1024]{1,0:T(8,128)}, u32[]{:S(2)}) copy-start(f32[16,1024]{1,0:T(8,128)} %get-tuple-element.87) | copy-start | bytes 196612
  171.0 56.7 %copy-start.5 = (f32[64,4,16]{2,1,0:T(4,128)}, f32[64,4,16]{2,1,0:T(4,128)S(1)}, u32[]{:S(2)}) copy-start(f32[64,4,16]{2,1,0:T(4,128)S(1)} %all-gather.1) | copy-start | bytes 49156
  207.4 20.3 %copy-start.6 = (f32[64,4,16]{2,1,0:T(4,128)}, f32[64,4,16]{2,1,0:T(4,128)S(1)}, u32[]{:S(2)}) copy-start(f32[64,4,16]{2,1,0:T(4,128)S(1)} %all-gather) | copy-start | bytes 49156
  211.5 3.4 copy-start.10
  211.5 3.5 copy-start.8
  214.9 3.5 copy-start.20
  214.9 5.5 %copy-start.14 = (f32[96]{0:T(128)S(1)}, f32[96]{0:T(128)}, u32[]{:S(2)}) copy-start(f32[96]{0:T(128)} %param.29) | copy-start | bytes 1156
  274.6 3.0 slice-start
  274.6 3.0 slice-start.1
  307.3 4.1 %copy-start.4 = (bf16[1024,256]{1,0:T(8,128)(2,1)S(1)}, bf16[1024,256]{1,0:T(8,128)(2,1)}, u32[]{:S(2)}) copy-start(bf16[1024,256]{1,0:T(8,128)(2,1)} %param.32) | copy-start | bytes 1572868
  307.3 46.6 %copy-start.11 = (f32[256]{0:T(256)S(1)}, f32[256]{0:T(256)}, u32[]{:S(2)}) copy-start(f32[256]{0:T(256)} %param.33) | copy-start | bytes 3076
Sparse Core Ops, SparseCore 0:
  14.1 110.8 all-reduce.2
  215.0 58.6 all-gather.4
where the time goes:
time: 363 us; the launch traced here: 361 us
  waiting for transfers between devices  144 us (40%)
  blocking collectives  118 us (33%)
  local copies, waits for them, and re-layouts  33.5 us (9%)
  matrix products  29.7 us (8%)
  other arithmetic  21.4 us (6%)
  between operations  14.5 us (4%)
    psum x1, waiting for transfers between devices, body(): query_raw, latent_raw = lax.psum((query_part, latent_part), 'kv')  97.9 us
    all_gather x2, blocking collectives, combined_all(): pieces = jax.tree.map(lambda part: lax.all_gather(part, axis), value)  75.8 us
    all_gather x1, waiting for transfers between devices, combined_all(): pieces = jax.tree.map(lambda part: lax.all_gather(part, axis), value)  46 us
    psum x1, blocking collectives, body(): squares = lax.psum(jnp.sum(projected * projected, -1), 'kv')  38.9 us
    dynamic_slice x15, local copies, waits for them, and re-layouts, combined_all(): lax.scan(lambda running, piece: (join(running, piece), None), head, tail)  13.9 us
    add x16, other arithmetic, combine(): left_total * left_scale + right_total * right_scale  10.9 us
    dot_general x2, matrix products, split_keys(): nope = jnp.dot(latents, w_key_up, preferred_element_type=jnp.float32)  7.4 us
    dot_general x2, matrix products, to_values(): jnp.einsum('sphc,chd->sphd', summed, value_up, precision=lax.Precision.HI...  7.28 us
  transfers between devices with their start and end apart: 2, of which 2 were waited for; matrix products, arithmetic and copies ran while one was open for 7% of the time, Pallas kernels for 0%

commit v1 on v0

--- a/solution.py
+++ b/solution.py
@@ -1,7 +1,14 @@
+import functools
+
 import jax
 import jax.numpy as jnp
+import numpy as np
 from jax import lax
+from jax.experimental import pallas as pl
+from jax.experimental.pallas import tpu as pltpu
 from jax.sharding import PartitionSpec as P
+
+MESH = pl.DeviceIdType.MESH
 
 D = 4096
 NOPE = 64
@@ -192,9 +199,407 @@
     return (mixed.reshape(seq_count, prop_count, -1), new_latent, new_rope)
 
 
+LANES = 128
+F32 = jnp.float32
+BF16 = jnp.bfloat16
+NT = (((1,), (1,)), ((), ()))
+TN = (((0,), (1,)), ((), ()))
+
+
+def lane_of(shape):
+    return lax.broadcasted_iota(jnp.int32, shape, len(shape) - 1)
+
+
+def row_of(shape):
+    return lax.broadcasted_iota(jnp.int32, shape, len(shape) - 2)
+
+
+def fold(top, bottom, low):
+    return jnp.where(low, top, pltpu.roll(bottom, 64, 1))
+
+
+def unfold_pair(first, second, low):
+    top = jnp.where(low, first, pltpu.roll(second, 64, 1))
+    bottom = jnp.where(low, pltpu.roll(first, 64, 1), second)
+    return jnp.concatenate([top, bottom], 0)
+
+
+def fused_kernel(
+    n, seqs, props, shard_len, width,
+    parents, lengths, accepted,
+    tokens, in_gain, latent_gain, query_gain, key_gain, out_gain, inverse,
+    wq_h, wl_h, wr_h, wk_h, wv_h, wo_h, cache_h, rope_h,
+    mixed_o, latent_o, rope_o,
+    wq, wl, wr, wk, wv, wo, cache, rope,
+    x_s, normed_s, keys_s, vhi_s, vlo_s,
+    send_a, recv_a, all_a, send_b, recv_b, all_b, proj_s, proj_in, sq_all,
+    out_lat, out_rope,
+    load_sem, store_sem, ssem, rsem, tsem,
+):
+    me = lax.axis_index("kv")
+    core = lax.axis_index("tp")
+    rows = seqs * props
+    heads = n
+    places = seqs * shard_len
+
+    loads = []
+    for at, (src, dst) in enumerate(
+        ((wq_h, wq), (wl_h, wl), (cache_h, cache), (rope_h, rope), (wk_h, wk), (wv_h, wv), (wr_h, wr), (wo_h, wo))
+    ):
+        load = pltpu.make_async_copy(src, dst, load_sem.at[at])
+        load.start()
+        loads.append(load)
+
+    barrier = pltpu.get_barrier_semaphore()
+    for off in range(1, n):
+        pl.semaphore_signal(barrier, inc=1, device_id=(lax.rem(me + off, n), core), device_id_type=MESH)
+    pl.semaphore_signal(barrier, inc=1, device_id=(me, 1 - core), device_id_type=MESH)
+
+    def copy_to(phase, off, src, dst):
+        return pltpu.make_async_remote_copy(
+            src_ref=src, dst_ref=dst, send_sem=ssem.at[phase, off], recv_sem=rsem.at[phase, off],
+            device_id=(lax.rem(me + off, n), core), device_id_type=MESH,
+        )
+
+    def scatter(phase, send, recv):
+        for off in range(1, n):
+            copy_to(phase, off, send.at[lax.rem(me + off, n)], recv.at[off]).start()
+
+    def scatter_wait(phase, off, send, recv):
+        copy_to(phase, off, send.at[lax.rem(me + off, n)], recv.at[off]).wait()
+
+    def gather(phase, table):
+        for off in range(1, n):
+            copy_to(phase, off, table.at[me], table.at[me]).start()
+
+    def gather_wait(phase, table):
+        for off in range(1, n):
+            copy_to(phase, off, table.at[me], table.at[lax.rem(me - off + n, n)]).wait_recv()
+        for off in range(1, n):
+            copy_to(phase, off, table.at[me], table.at[me]).wait_send()
+
+    for s in range(seqs):
+        x_s[s * props : (s + 1) * props, :] = tokens[s].astype(F32)
+    x = x_s[...]
+    normed_s[...] = (x * lax.rsqrt(jnp.mean(x * x, -1, keepdims=True) + epsilon) * in_gain[...]).astype(BF16)
+    part_rows = wq.shape[0]
+    part = normed_s[:, pl.ds(pl.multiple_of(me * part_rows, part_rows), part_rows)]
+    loads[0].wait()
+    q_part = jnp.dot(part, wq[...], preferred_element_type=F32)
+    loads[1].wait()
+    l_part = jnp.dot(part, wl[...], preferred_element_type=F32)
+    low8 = lane_of((8, LANES)) < 64
+    for h in range(heads):
+        if h < heads - 1:
+            piece = q_part[:, h * QK : h * QK + LANES]
+        else:
+            piece = jnp.concatenate([q_part[:, h * QK :], jnp.zeros((rows, LANES - QK), F32)], 1)
+        send_a[h, 0:rows, :] = piece
+    for m in range(n // 2):
+        top = l_part[0:8, m * LANES : (m + 1) * LANES]
+        bottom = l_part[8:16, m * LANES : (m + 1) * LANES]
+        send_a[2 * m, rows : rows + 8, :] = fold(top, bottom, low8)
+        send_a[2 * m + 1, rows : rows + 8, :] = jnp.where(low8, pltpu.roll(top, 64, 1), bottom)
+    pl.semaphore_wait(barrier, n)
+    scatter(0, send_a, recv_a)
+
+    lane = lane_of((rows, LANES))
+    row = row_of((rows, LANES))
+    anchors = [lengths[s] + accepted[s] for s in range(seqs)]
+    position = jnp.zeros((rows, LANES), jnp.int32)
+    seen_own = jnp.zeros((rows, LANES), jnp.int32)
+    for s in range(seqs):
+        table = []
+        for i in range(props):
+            line = []
+            for j in range(props):
+                if j > i:
+                    line.append(None)
+                elif j == i:
+                    line.append(jnp.int32(1))
+                else:
+                    hit = jnp.int32(0)
+                    for m in range(j, i):
+                        hit = hit + jnp.where(parents[s, i] == m, table[m][j], 0)
+                    line.append(hit)
+            table.append(line)
+            at = anchors[s] + sum(line[1 : i + 1], line[0]) - 1
+            position = jnp.where(row == s * props + i, at, position)
+            for j in range(i + 1):
+                here = (row == s * props + i) & (lane == s * props + j)
+                seen_own = jnp.where(here, line[j], seen_own)
+    angle = position.astype(F32) * inverse[...]
+    cosine = jnp.cos(angle)
+    sine = jnp.where(lane < NOPE + ROPE // 2, -jnp.sin(angle), jnp.sin(angle))
+
+    groups = heads // 4
+    pad = jnp.zeros((1, LANES - QK), F32)
+    key_gain_row = jnp.concatenate([key_gain[...], pad], 1)
+    gain_col = jnp.transpose(jnp.broadcast_to(key_gain_row, (LANES, LANES)))[:, 0:1]
+    loads[2].wait()
+    loads[3].wait()
+    loads[4].wait()
+    cached = cache[...].reshape(places, width)
+    eye = (row_of((ROPE, ROPE)) == lane_of((ROPE, ROPE))).astype(BF16)
+    rope_t = lax.dot_general(eye, rope[...].reshape(places, ROPE), NT, preferred_element_type=F32)
+    rope_sq = jnp.sum(rope_t * rope_t, 0, keepdims=True)
+    rope_gained = gain_col[NOPE:QK, :]
+    for g in range(groups):
+        nope_t = lax.dot_general(wk[:, g * 256 : (g + 1) * 256], cached, TN, preferred_element_type=F32)
+        for j in range(4):
+            nope = nope_t[j * NOPE : (j + 1) * NOPE, :]
+            factor = lax.rsqrt((jnp.sum(nope * nope, 0, keepdims=True) + rope_sq) / QK + epsilon)
+            keys_s[g, j * NOPE : (j + 1) * NOPE, :] = (nope * factor * gain_col[0:NOPE, :]).astype(BF16)
+            keys_s[g, 256 + j * ROPE : 256 + (j + 1) * ROPE, :] = (rope_t * factor * rope_gained).astype(BF16)
+
+    total = send_a[me]
+    for off in range(1, n):
+        scatter_wait(0, off, send_a, recv_a)
+        total = total + recv_a[off]
+    q = jnp.where(lane < QK, total[0:rows], 0.0)
+    half = ROPE // 2
+
+    def turn(v, cos, sin, split):
+        other = jnp.where(lane < split, pltpu.roll(v, LANES - half, 1), pltpu.roll(v, half, 1))
+        return v * cos + other * sin
+
+    q = turn(q, cosine, sine, NOPE + half)
+    q = jnp.where(lane < QK, q, 0.0)
+    query_gain_row = jnp.concatenate([query_gain[...], pad], 1)
+    q = q * lax.rsqrt(jnp.sum(q * q, -1, keepdims=True) / QK + epsilon) * query_gain_row
+    my_query = q.astype(BF16)
+    all_a[me, 0:rows, :] = my_query.astype(F32)
+    all_a[me, rows : rows + 8, :] = total[rows : rows + 8]
+    gather(1, all_a)
+
+    loads[5].wait()
+    for g in range(groups):
+        value = jnp.dot(cached, wv[:, g * 256 : (g + 1) * 256], preferred_element_type=F32)
+        high = value.astype(BF16)
+        vhi_s[:, g * 256 : (g + 1) * 256] = high
+        vlo_s[:, g * 256 : (g + 1) * 256] = (value - high.astype(F32)).astype(BF16)
+    loads[6].wait()
+    rope_raw = jnp.dot(normed_s[...], wr[...], preferred_element_type=F32)
+    rope_raw = jnp.concatenate([rope_raw, jnp.zeros((rows, LANES - ROPE), F32)], 1)
+    rope_new = turn(rope_raw, pltpu.roll(cosine, 64, 1), pltpu.roll(sine, 64, 1), half)
+    rope_new = jnp.where(lane < ROPE, rope_new, 0.0).astype(BF16)
+
+    gather_wait(1, all_a)
+    tall = 4 * rows
+    row4 = row_of((tall, LANES))
+    lane4 = lane_of((tall, LANES))
+    seq4 = lax.rem(row4, rows) // props
+    anchor4 = jnp.zeros((tall, LANES), jnp.int32)
+    for s in range(seqs):
+        anchor4 = jnp.where(seq4 == s, anchors[s], anchor4)
+    seen = me * shard_len + lane4 < anchor4
+    head4 = row4 // rows
+    for g in range(groups):
+        parts = [all_a[4 * g + j, 0:rows, :] for j in range(4)]
+        stacked = jnp.concatenate(parts, 0)
+        twice = jnp.where(lane4 < 64, stacked, pltpu.roll(stacked, 64, 1))
+        halves = [jnp.where(head4 == 2 * c + lane4 // 64, twice, 0.0) for c in range(2)]
+        turned = jnp.concatenate([pltpu.roll(parts[j], (64 + 32 * j) % LANES, 1) if j != 2 else parts[j] for j in range(4)], 0)
+        turned = jnp.where(head4 == lane4 // ROPE, turned, 0.0)
+        wide_q = jnp.concatenate(halves + [turned], 1).astype(BF16)
+        scores = jnp.dot(wide_q, keys_s[g], preferred_element_type=F32)
+        mine = scores[:, 0:shard_len]
+        for s in range(1, seqs):
+            mine = jnp.where(seq4 == s, scores[:, s * shard_len : (s + 1) * shard_len], mine)
+        mine = jnp.where(seen, mine * QK ** (-0.5), -1e30)
+        peak = jnp.max(mine, -1, keepdims=True)
+        weights = jnp.where(seen, jnp.exp(mine - peak), 0.0)
+        totals = jnp.sum(weights, -1, keepdims=True)
+        spread = jnp.concatenate([jnp.where(seq4 == s, weights, 0.0) for s in range(seqs)], 1).astype(BF16)
+        summed = jnp.dot(spread, vhi_s[:, g * 256 : (g + 1) * 256], preferred_element_type=F32)
+        summed = summed + jnp.dot(spread, vlo_s[:, g * 256 : (g + 1) * 256], preferred_element_type=F32)
+        for j in range(4):
+            block = slice(j * rows, (j + 1) * rows)
+            here = summed[block, (j // 2) * LANES : (j // 2 + 1) * LANES]
+            if j % 2:
+                here = pltpu.roll(here, 64, 1)
+            send_b[4 * g + j] = jnp.where(lane < 64, here, jnp.where(lane < 96, peak[block], totals[block]))
+    scatter(2, send_b, recv_b)
+
+    latent = jnp.concatenate(
+        [unfold_pair(all_a[2 * m, rows : rows + 8, :], all_a[2 * m + 1, rows : rows + 8, :], low8) for m in range(n // 2)], 1
+    )
+    latent_new = (
+        latent * lax.rsqrt(jnp.mean(latent * latent, -1, keepdims=True) + epsilon) * latent_gain[...]
+    ).astype(BF16)
+
+    pair = pl.ds(pl.multiple_of((me // 2) * LANES, LANES), LANES)
+    odd = jnp.broadcast_to(lax.rem(me, 2), (rows, LANES)) == 1
+
+    def of_head(both):
+        return jnp.where(odd, pltpu.roll(both, 64, 1), both)
+
+    own_nope = of_head(jnp.dot(latent_new, wk[:, pair], preferred_element_type=F32))
+    own_key = jnp.where(lane < NOPE, own_nope, pltpu.roll(rope_new.astype(F32), 64, 1))
+    own_key = jnp.where(lane < QK, own_key, 0.0)
+    own_key = own_key * lax.rsqrt(jnp.sum(own_key * own_key, -1, keepdims=True) / QK + epsilon) * key_gain_row
+    own_scores = lax.dot_general(
+        my_query, jnp.concatenate([own_key, jnp.zeros((LANES - rows, LANES), F32)], 0).astype(BF16),
+        NT, preferred_element_type=F32,
+    )
+    own_seen = seen_own > 0
+    own_scores = jnp.where(own_seen, own_scores * QK ** (-0.5), -1e30)
+    own_peak = jnp.max(own_scores, -1, keepdims=True)
+    own_weights = jnp.where(own_seen, jnp.exp(own_scores - own_peak), 0.0)
+    own_total = jnp.sum(own_weights, -1, keepdims=True)
+    own_value = of_head(jnp.dot(latent_new, wv[:, pair], preferred_element_type=F32))
+    own_value = jnp.concatenate([own_value, jnp.zeros((LANES - rows, LANES), F32)], 0)
+    own_high = own_value.astype(BF16)
+    own_low = (own_value - own_high.astype(F32)).astype(BF16)
+    own_low_weights = own_weights.astype(BF16)
+    own_sum = jnp.dot(own_low_weights, own_high, preferred_element_type=F32)
+    own_sum = own_sum + jnp.dot(own_low_weights, own_low, preferred_element_type=F32)
+
+    slot = lane_of((shard_len, rows))
+    stores = []
+    for s in range(seqs):
+        offset = me * shard_len + row_of((shard_len, rows)) - anchors[s]
+        chosen = ((slot // props == s) & (offset == lax.rem(slot, props))).astype(F32).astype(BF16)
+        put = jnp.dot(chosen, latent_new, preferred_element_type=F32)
+        wide = me * shard_len + row_of((shard_len, width)) - anchors[s]
+        filled = (wide >= 0) & (wide < props)
+        out_lat[s] = jnp.where(filled, put, cache[s].astype(F32)).astype(BF16)
+        put_rope = jnp.dot(chosen, rope_new, preferred_element_type=F32)[:, 0:ROPE]
+        thin = me * shard_len + row_of((shard_len, ROPE)) - anchors[s]
+        out_rope[s] = jnp.where((thin >= 0) & (thin < props), put_rope, rope[s].astype(F32)).astype(BF16)
+    for at, (src, dst) in enumerate(((out_lat, latent_o), (out_rope, rope_o))):
+        store = pltpu.make_async_copy(src, dst, store_sem.at[at])
+        store.start()
+        stores.append(store)
+
+    pieces = [send_b[me]]
+    for off in range(1, n):
+        scatter_wait(2, off, send_b, recv_b)
+        pieces.append(recv_b[off])
+    peaks = [piece[:, 64:65] for piece in pieces]
+    highest = own_peak
+    for peak in peaks:
+        highest = jnp.maximum(highest, peak)
+    scale = jnp.exp(own_peak - highest)
+    joint_sum = own_sum * scale
+    joint_total = own_total * scale
+    for piece, peak in zip(pieces, peaks):
+        scale = jnp.exp(peak - highest)
+        joint_sum = joint_sum + piece * scale
+        joint_total = joint_total + piece[:, 96:97] * scale
+    values_low = (joint_sum / joint_total).astype(BF16).astype(F32)
+    all_b[me] = fold(values_low[0:8], values_low[8:16], low8)
+    gather(3, all_b)
+    loads[7].wait()
+    gather_wait(3, all_b)
+    values = jnp.concatenate(
+        [unfold_pair(all_b[2 * m], all_b[2 * m + 1], low8) for m in range(n // 2)], 1
+    ).astype(BF16)
+
+    proj_s[...] = jnp.dot(values, wo[...], preferred_element_type=F32)
+    swap = pltpu.make_async_remote_copy(
+        src_ref=proj_s, dst_ref=proj_in, send_sem=tsem.at[0], recv_sem=tsem.at[1],
+        device_id=(me, 1 - core), device_id_type=MESH,
+    )
+    swap.start()
+    swap.wait()
+    projected = proj_s[...] + proj_in[...]
+    squares = jnp.broadcast_to(jnp.sum(projected * projected, -1, keepdims=True), (rows, LANES))
+    sq_all[me] = jnp.where(low8, squares[0:8], squares[8:16])
+    gather(4, sq_all)
+    gather_wait(4, sq_all)
+    squares = sq_all[0]
+    for k in range(1, n):
+        squares = squares + sq_all[k]
+    squares = jnp.concatenate([squares[:, 0:1], squares[:, 64:65]], 0)
+    model_width = x_s.shape[1]
+    mixed = (projected * lax.rsqrt(squares / model_width + epsilon) * out_gain[...]).astype(BF16)
+    for s in range(seqs):
+        mixed_o[s] = mixed[s * props : (s + 1) * props, :]
+    for store in stores:
+        store.wait()
+
+
+def fused(
+    n, tokens, parents, lengths, accepted, in_gain, w_query, w_latent, w_rope_key, latent_gain, query_gain,
+    key_gain, w_key_up, w_value_up, w_out, out_gain, cache_latent, cache_rope,
+):
+    seqs, props, model_width = tokens.shape
+    shard_len, width = cache_latent.shape[1:]
+    rows = seqs * props
+    places = seqs * shard_len
+    heads_wide = w_value_up.shape[1]
+    out_cols = w_out.shape[1]
+    half = ROPE // 2
+    wave = rope_base ** (-np.arange(half, dtype=np.float32) / np.float32(half))
+    inverse = np.zeros((1, LANES), np.float32)
+    inverse[0, NOPE : NOPE + half] = wave
+    inverse[0, NOPE + half : QK] = wave
+    smem = pl.BlockSpec(memory_space=pltpu.SMEM)
+    vmem = pl.BlockSpec(memory_space=pltpu.VMEM)
+    hbm = pl.BlockSpec(memory_space=pl.ANY)
+    held = [w_query, w_latent, w_rope_key, w_key_up, w_value_up, w_out, cache_latent, cache_rope]
+    return pl.pallas_call(
+        functools.partial(fused_kernel, n, seqs, props, shard_len, width),
+        out_shape=(
+            jax.ShapeDtypeStruct((seqs, props, out_cols), BF16),
+            jax.ShapeDtypeStruct(cache_latent.shape, BF16),
+            jax.ShapeDtypeStruct(cache_rope.shape, BF16),
+        ),
+        in_specs=[smem] * 3 + [vmem] * 7 + [hbm] * 8,
+        out_specs=(vmem, hbm, hbm),
+        scratch_shapes=[pltpu.VMEM(array.shape, array.dtype) for array in held]
+        + [
+            pltpu.VMEM((rows, model_width), F32),
+            pltpu.VMEM((rows, model_width), BF16),
+            pltpu.VMEM((n // 4, 4 * QK, places), BF16),
+            pltpu.VMEM((places, heads_wide), BF16),
+            pltpu.VMEM((places, heads_wide), BF16),
+            pltpu.VMEM((n, rows + 8, LANES), F32),
+            pltpu.VMEM((n, rows + 8, LANES), F32),
+            pltpu.VMEM((n, rows + 8, LANES), F32),
+            pltpu.VMEM((n, rows, LANES), F32),
+            pltpu.VMEM((n, rows, LANES), F32),
+            pltpu.VMEM((n, 8, LANES), F32),
+            pltpu.VMEM((rows, out_cols), F32),
+            pltpu.VMEM((rows, out_cols), F32),
+            pltpu.VMEM((n, 8, LANES), F32),
+            pltpu.VMEM(cache_latent.shape, BF16),
+            pltpu.VMEM(cache_rope.shape, BF16),
+            pltpu.SemaphoreType.DMA((len(held),)),
+            pltpu.SemaphoreType.DMA((2,)),
+            pltpu.SemaphoreType.DMA((5, n)),
+            pltpu.SemaphoreType.DMA((5, n)),
+            pltpu.SemaphoreType.DMA((2,)),
+        ],
+        compiler_params=pltpu.CompilerParams(
+            collective_id=0, has_side_effects=True, vmem_limit_bytes=56 * 1024 * 1024
+        ),
+    )(
+        parents, lengths, accepted, tokens, in_gain.reshape(1, -1), latent_gain.reshape(1, -1),
+        query_gain.reshape(1, -1), key_gain.reshape(1, -1), out_gain.reshape(1, -1), jnp.asarray(inverse), *held,
+    )
+
+
+def step(n, cores, tokens, *others):
+    w_query, w_latent, w_key_up, cache_latent = others[4], others[5], others[10], others[14]
+    fits = (
+        tokens.shape[0] * tokens.shape[1] == 16
+        and cores == 2
+        and w_key_up.shape[1] == n * NOPE
+        and w_latent.shape[1] == n * 64
+        and n % 4 == 0
+        and w_query.shape[0] % LANES == 0
+        and cache_latent.shape[1] == LANES
+    )
+    if fits:
+        return fused(n, tokens, *others)
+    return body(tokens, *others)
+
+
 def solution(mesh):
     return jax.shard_map(
-        body,
+        functools.partial(step, mesh.shape["kv"], mesh.shape["tp"]),
         mesh=mesh,
         in_specs=(
             P(),

time: 363 us -> 48.9 us (0.13)
  waiting for transfers between devices: 144 us -> 0 us
  blocking collectives: 118 us -> 0 us
  Pallas kernels: 0 us -> 39 us
  matrix products: 29.7 us -> 0 us
  local copies, waits for them, and re-layouts: 33.5 us -> 8.94 us
  other arithmetic: 21.4 us -> 0 us
  between operations: 14.5 us -> 0.64 us
    psum x1 -> x0, waiting for transfers between devices: 97.9 us -> none  [body(): query_raw, latent_raw = lax.psum((query_part, latent_part), 'kv')]
    all_gather x2 -> x0, blocking collectives: 75.8 us -> none  [combined_all(): pieces = jax.tree.map(lambda part: lax.all_gather(part, axis), value)]
    all_gather x1 -> x0, waiting for transfers between devices: 46 us -> none  [combined_all(): pieces = jax.tree.map(lambda part: lax.all_gather(part, axis), value)]
    psum x2 -> x0, blocking collectives: 42.3 us -> none  [the longest x1 38.9 us: body(): squares = lax.psum(jnp.sum(projected * projected, -1), 'kv')]
    pallas_call x0 -> x1, Pallas kernels: none -> 39 us  [fused(): pl.pallas_call(functools.partial(fused_kernel, n, seqs, props, shard_len,...]
    dot_general x19 -> x0, matrix products: 29.7 us -> none  [the longest x2 7.4 us: split_keys(): nope = jnp.dot(latents, w_key_up, preferred_element_type=jnp.float32)]
    dynamic_slice x16 -> x0, local copies, waits for them, and re-layouts: 14.6 us -> none  [the longest x15 13.9 us: combined_all(): lax.scan(lambda running, piece: (join(running, piece), None), head, tail)]
    add x33 -> x0, other arithmetic: 13.3 us -> none  [the longest x16 10.9 us: combine(): left_total * left_scale + right_total * right_scale]
  transfers between devices with their start and end apart: 2 -> 0, of which waited for: 2 -> 0; matrix products, arithmetic and copies ran while one was open for 7% -> 0% of each run, Pallas kernels for 0% -> 0%
where the time goes in v1:
time: 48.9 us; the launch traced here: 48.6 us
  Pallas kernels  39 us (80%)
  local copies, waits for them, and re-layouts  8.94 us (18%)
  between operations  0.64 us (1%)
    pallas_call x1, Pallas kernels, fused(): pl.pallas_call(functools.partial(fused_kernel, n, seqs, props, shard_len,...  39 us
    unnamed x4, local copies, waits for them, and re-layouts  7.34 us
    pallas_call x1, local copies, waits for them, and re-layouts, fused(): pl.pallas_call(functools.partial(fused_kernel, n, seqs, props, shard_len,...  1.6 us

profile of v1, /device:TPU:0, one launch (start us, length us, event | category | flops | bytes accessed | tf_op | source)
XLA Modules:
  0.0 48.6 jit_solution(11020204407238643510)
XLA Ops:
  0.6 1.5 %copy.22.rope_h = bf16[4,128,32]{2,1,0:T(8,128)(2,1)} copy(bf16[4,128,32]{1,2,0:T(8,128)(2,1)} %param.34) | data formatting | bytes 65536 | tf_op args[16]
  2.1 2.3 %copy.21.wr_h = bf16[4096,32]{1,0:T(8,128)(2,1)} copy(bf16[4096,32]{0,1:T(8,128)(2,1)} %param.25) | data formatting | bytes 524288 | tf_op args[7]
  4.4 39.0 %shard_map.193 = (bf16[4,4,256]{2,1,0:T(4,128)(2,1)}, bf16[4,128,1024]{2,1,0:T(8,128)(2,1)}, bf16[4,128,32]{2,1,0:T(8,128)(2,1)}) custom-call(s32[4,4]{1,0:T(4,128)} %parents.1, s32[4]{0:T(128)} %lengths.1, s32[4]{0:T(128)} %accepted.1, bf16[4,4,4096]{2,1,0:T(4,128)(2,1)} %tokens.1, f32[1,4096]{1,0:T(1,128)} %bitcast.5, f32[1,1024]{1,0:T(1,128)} %bitcast.6, ...), custom_call_target="tpu_custom_call" | custom-call | tf_op jit(solution)/shard_map/pallas_call | solution.py:542
  43.4 1.6 %copy.23 = bf16[4,128,32]{1,2,0:T(8,128)(2,1)} copy(bf16[4,128,32]{2,1,0:T(8,128)(2,1)} %get-tuple-element.5) | data formatting | bytes 65536 | tf_op jit(solution)/shard_map/pallas_call | solution.py:542
  45.0 1.3 %copy.26 = bf16[4,4,256]{2,1,0:T(4,128)(2,1)} copy(bf16[4,4,256]{2,1,0:T(4,128)(2,1)} %get-tuple-element.9) | data formatting | bytes 16384
  46.3 2.3 %copy.27 = bf16[4,128,1024]{2,1,0:T(8,128)(2,1)} copy(bf16[4,128,1024]{2,1,0:T(8,128)(2,1)} %get-tuple-element.10) | data formatting | bytes 2097152

commit v2 on v1

--- a/solution.py
+++ b/solution.py
@@ -232,9 +232,8 @@
     mixed_o, latent_o, rope_o,
     wq, wl, wr, wk, wv, wo, cache, rope,
     x_s, normed_s, keys_s, vhi_s, vlo_s,
-    send_a, recv_a, all_a, send_b, recv_b, all_b, proj_s, proj_in, sq_all,
-    out_lat, out_rope,
-    load_sem, store_sem, ssem, rsem, tsem,
+    send_a, recv_a, all_a, send_b, recv_b, all_b, proj_s, proj_in, sq_all, lat_s,
+    load_sem, ssem, rsem, tsem,
 ):
     me = lax.axis_index("kv")
     core = lax.axis_index("tp")
@@ -242,6 +241,7 @@
     heads = n
     places = seqs * shard_len
 
+    order = sorted(range(1, n), key=lambda off: abs(off - n // 2))
     loads = []
     for at, (src, dst) in enumerate(
         ((wq_h, wq), (wl_h, wl), (cache_h, cache), (rope_h, rope), (wk_h, wk), (wv_h, wv), (wr_h, wr), (wo_h, wo))
@@ -251,7 +251,7 @@
         loads.append(load)
 
     barrier = pltpu.get_barrier_semaphore()
-    for off in range(1, n):
+    for off in order:
         pl.semaphore_signal(barrier, inc=1, device_id=(lax.rem(me + off, n), core), device_id_type=MESH)
     pl.semaphore_signal(barrier, inc=1, device_id=(me, 1 - core), device_id_type=MESH)
 
@@ -262,20 +262,20 @@
         )
 
     def scatter(phase, send, recv):
-        for off in range(1, n):
+        for off in order:
             copy_to(phase, off, send.at[lax.rem(me + off, n)], recv.at[off]).start()
 
     def scatter_wait(phase, off, send, recv):
         copy_to(phase, off, send.at[lax.rem(me + off, n)], recv.at[off]).wait()
 
     def gather(phase, table):
-        for off in range(1, n):
+        for off in order:
             copy_to(phase, off, table.at[me], table.at[me]).start()
 
     def gather_wait(phase, table):
-        for off in range(1, n):
+        for off in order:
             copy_to(phase, off, table.at[me], table.at[lax.rem(me - off + n, n)]).wait_recv()
-        for off in range(1, n):
+        for off in order:
             copy_to(phase, off, table.at[me], table.at[me]).wait_send()
 
     for s in range(seqs):
@@ -288,23 +288,25 @@
     q_part = jnp.dot(part, wq[...], preferred_element_type=F32)
     loads[1].wait()
     l_part = jnp.dot(part, wl[...], preferred_element_type=F32)
+    lane = lane_of((rows, LANES))
+    row = row_of((rows, LANES))
     low8 = lane_of((8, LANES)) < 64
+    first_core = jnp.broadcast_to(core, (8, width)) == 0
+    l_half = jnp.where(first_core, l_part[0:8], l_part[8:16])
     for h in range(heads):
         if h < heads - 1:
             piece = q_part[:, h * QK : h * QK + LANES]
         else:
             piece = jnp.concatenate([q_part[:, h * QK :], jnp.zeros((rows, LANES - QK), F32)], 1)
-        send_a[h, 0:rows, :] = piece
-    for m in range(n // 2):
-        top = l_part[0:8, m * LANES : (m + 1) * LANES]
-        bottom = l_part[8:16, m * LANES : (m + 1) * LANES]
-        send_a[2 * m, rows : rows + 8, :] = fold(top, bottom, low8)
-        send_a[2 * m + 1, rows : rows + 8, :] = jnp.where(low8, pltpu.roll(top, 64, 1), bottom)
+        both = l_half[:, (h // 2) * LANES : (h // 2 + 1) * LANES]
+        if h % 2:
+            rest = [pltpu.roll(both, 32, 1), both]
+        else:
+            rest = [pltpu.roll(both, 96, 1), pltpu.roll(both, 64, 1)]
+        send_a[h] = jnp.where(lane < QK, piece, jnp.concatenate(rest, 0))
     pl.semaphore_wait(barrier, n)
     scatter(0, send_a, recv_a)
 
-    lane = lane_of((rows, LANES))
-    row = row_of((rows, LANES))
     anchors = [lengths[s] + accepted[s] for s in range(seqs)]
     position = jnp.zeros((rows, LANES), jnp.int32)
     seen_own = jnp.zeros((rows, LANES), jnp.int32)
@@ -340,8 +342,7 @@
     loads[3].wait()
     loads[4].wait()
     cached = cache[...].reshape(places, width)
-    eye = (row_of((ROPE, ROPE)) == lane_of((ROPE, ROPE))).astype(BF16)
-    rope_t = lax.dot_general(eye, rope[...].reshape(places, ROPE), NT, preferred_element_type=F32)
+    rope_t = jnp.concatenate([rope[s].astype(F32) for s in range(seqs)], 1)
     rope_sq = jnp.sum(rope_t * rope_t, 0, keepdims=True)
     rope_gained = gain_col[NOPE:QK, :]
     for g in range(groups):
@@ -353,10 +354,10 @@
             keys_s[g, 256 + j * ROPE : 256 + (j + 1) * ROPE, :] = (rope_t * factor * rope_gained).astype(BF16)
 
     total = send_a[me]
-    for off in range(1, n):
+    for off in reversed(order):
         scatter_wait(0, off, send_a, recv_a)
         total = total + recv_a[off]
-    q = jnp.where(lane < QK, total[0:rows], 0.0)
+    q = jnp.where(lane < QK, total, 0.0)
     half = ROPE // 2
 
     def turn(v, cos, sin, split):
@@ -368,8 +369,7 @@
     query_gain_row = jnp.concatenate([query_gain[...], pad], 1)
     q = q * lax.rsqrt(jnp.sum(q * q, -1, keepdims=True) / QK + epsilon) * query_gain_row
     my_query = q.astype(BF16)
-    all_a[me, 0:rows, :] = my_query.astype(F32)
-    all_a[me, rows : rows + 8, :] = total[rows : rows + 8]
+    all_a[me] = jnp.where(lane < QK, my_query.astype(F32), total)
     gather(1, all_a)
 
     loads[5].wait()
@@ -379,7 +379,7 @@
         vhi_s[:, g * 256 : (g + 1) * 256] = high
         vlo_s[:, g * 256 : (g + 1) * 256] = (value - high.astype(F32)).astype(BF16)
     loads[6].wait()
-    rope_raw = jnp.dot(normed_s[...], wr[...], preferred_element_type=F32)
+    rope_raw = lax.dot_general(normed_s[...], wr[...], NT, preferred_element_type=F32)
     rope_raw = jnp.concatenate([rope_raw, jnp.zeros((rows, LANES - ROPE), F32)], 1)
     rope_new = turn(rope_raw, pltpu.roll(cosine, 64, 1), pltpu.roll(sine, 64, 1), half)
     rope_new = jnp.where(lane < ROPE, rope_new, 0.0).astype(BF16)
@@ -395,7 +395,7 @@
     seen = me * shard_len + lane4 < anchor4
     head4 = row4 // rows
     for g in range(groups):
-        parts = [all_a[4 * g + j, 0:rows, :] for j in range(4)]
+        parts = [all_a[4 * g + j] for j in range(4)]
         stacked = jnp.concatenate(parts, 0)
         twice = jnp.where(lane4 < 64, stacked, pltpu.roll(stacked, 64, 1))
         halves = [jnp.where(head4 == 2 * c + lane4 // 64, twice, 0.0) for c in range(2)]
@@ -421,9 +421,24 @@
             send_b[4 * g + j] = jnp.where(lane < 64, here, jnp.where(lane < 96, peak[block], totals[block]))
     scatter(2, send_b, recv_b)
 
-    latent = jnp.concatenate(
-        [unfold_pair(all_a[2 * m, rows : rows + 8, :], all_a[2 * m + 1, rows : rows + 8, :], low8) for m in range(n // 2)], 1
-    )
+    lane8 = lane_of((8, LANES))
+    blocks = []
+    for m in range(n // 2):
+        even, odd_part = all_a[2 * m], all_a[2 * m + 1]
+        left = jnp.where(lane8 < 32, pltpu.roll(even[0:8], 32, 1), pltpu.roll(even[8:16], 64, 1))
+        right = jnp.where(lane8 < 96, pltpu.roll(odd_part[0:8], 96, 1), odd_part[8:16])
+        blocks.append(jnp.where(low8, left, right))
+    lat_s[core] = jnp.concatenate(blocks, 1)
+    pltpu.make_async_remote_copy(
+        src_ref=lat_s.at[core], dst_ref=lat_s.at[core], send_sem=tsem.at[2], recv_sem=tsem.at[3],
+        device_id=(me, 1 - core), device_id_type=MESH,
+    ).start()
+    arrived = pltpu.make_async_remote_copy(
+        src_ref=lat_s.at[core], dst_ref=lat_s.at[1 - core], send_sem=tsem.at[2], recv_sem=tsem.at[3],
+        device_id=(me, 1 - core), device_id_type=MESH,
+    )
+    arrived.wait()
+    latent = jnp.concatenate([lat_s[0], lat_s[1]], 0)
     latent_new = (
         latent * lax.rsqrt(jnp.mean(latent * latent, -1, keepdims=True) + epsilon) * latent_gain[...]
     ).astype(BF16)
@@ -455,25 +470,11 @@
     own_sum = jnp.dot(own_low_weights, own_high, preferred_element_type=F32)
     own_sum = own_sum + jnp.dot(own_low_weights, own_low, preferred_element_type=F32)
 
-    slot = lane_of((shard_len, rows))
-    stores = []
-    for s in range(seqs):
-        offset = me * shard_len + row_of((shard_len, rows)) - anchors[s]
-        chosen = ((slot // props == s) & (offset == lax.rem(slot, props))).astype(F32).astype(BF16)
-        put = jnp.dot(chosen, latent_new, preferred_element_type=F32)
-        wide = me * shard_len + row_of((shard_len, width)) - anchors[s]
-        filled = (wide >= 0) & (wide < props)
-        out_lat[s] = jnp.where(filled, put, cache[s].astype(F32)).astype(BF16)
-        put_rope = jnp.dot(chosen, rope_new, preferred_element_type=F32)[:, 0:ROPE]
-        thin = me * shard_len + row_of((shard_len, ROPE)) - anchors[s]
-        out_rope[s] = jnp.where((thin >= 0) & (thin < props), put_rope, rope[s].astype(F32)).astype(BF16)
-    for at, (src, dst) in enumerate(((out_lat, latent_o), (out_rope, rope_o))):
-        store = pltpu.make_async_copy(src, dst, store_sem.at[at])
-        store.start()
-        stores.append(store)
+    latent_o[...] = latent_new
+    rope_o[...] = rope_new
 
     pieces = [send_b[me]]
-    for off in range(1, n):
+    for off in reversed(order):
         scatter_wait(2, off, send_b, recv_b)
         pieces.append(recv_b[off])
     peaks = [piece[:, 64:65] for piece in pieces]
@@ -504,18 +505,50 @@
     swap.start()
     swap.wait()
     projected = proj_s[...] + proj_in[...]
-    squares = jnp.broadcast_to(jnp.sum(projected * projected, -1, keepdims=True), (rows, LANES))
-    sq_all[me] = jnp.where(low8, squares[0:8], squares[8:16])
+    squares = jnp.sum(projected * projected, -1, keepdims=True)
+    on_diagonal = row == lane
+    sq_all[me] = jnp.sum(jnp.where(on_diagonal, squares, 0.0), 0, keepdims=True)
     gather(4, sq_all)
     gather_wait(4, sq_all)
     squares = sq_all[0]
     for k in range(1, n):
         squares = squares + sq_all[k]
-    squares = jnp.concatenate([squares[:, 0:1], squares[:, 64:65]], 0)
+    squares = jnp.sum(jnp.where(on_diagonal, squares, 0.0), -1, keepdims=True)
     model_width = x_s.shape[1]
     mixed = (projected * lax.rsqrt(squares / model_width + epsilon) * out_gain[...]).astype(BF16)
     for s in range(seqs):
         mixed_o[s] = mixed[s * props : (s + 1) * props, :]
+
+
+def finish_kernel(
+    seqs, props, shard_len, width,
+    lengths, accepted, mixed, latent_new, rope_new, rope_in, cache_h,
+    mixed_o, rope_o, latent_o, cache, out_lat, load_sem, store_sem,
+):
+    me = lax.axis_index("kv")
+    rows = seqs * props
+    loads = [pltpu.make_async_copy(cache_h.at[s], cache.at[s], load_sem.at[s]) for s in range(seqs)]
+    for load in loads:
+        load.start()
+    mixed_o[...] = mixed[...]
+    slot = lane_of((shard_len, rows))
+    chosen = []
+    for s in range(seqs):
+        start = lengths[s] + accepted[s] - me * shard_len
+        offset = row_of((shard_len, rows)) - start
+        chosen.append(((slot // props == s) & (offset == lax.rem(slot, props))).astype(F32).astype(BF16))
+        put_rope = lax.dot_general(rope_new[...], chosen[s], TN, preferred_element_type=F32)[0:ROPE]
+        across = lane_of((ROPE, shard_len)) - start
+        rope_o[s] = jnp.where((across >= 0) & (across < props), put_rope, rope_in[s].astype(F32)).astype(BF16)
+    stores = []
+    for s in range(seqs):
+        put = jnp.dot(chosen[s], latent_new[...], preferred_element_type=F32)
+        down = row_of((shard_len, width)) - (lengths[s] + accepted[s] - me * shard_len)
+        loads[s].wait()
+        out_lat[s] = jnp.where((down >= 0) & (down < props), put, cache[s].astype(F32)).astype(BF16)
+        store = pltpu.make_async_copy(out_lat.at[s], latent_o.at[s], store_sem.at[s])
+        store.start()
+        stores.append(store)
     for store in stores:
         store.wait()
 
@@ -538,16 +571,17 @@
     smem = pl.BlockSpec(memory_space=pltpu.SMEM)
     vmem = pl.BlockSpec(memory_space=pltpu.VMEM)
     hbm = pl.BlockSpec(memory_space=pl.ANY)
-    held = [w_query, w_latent, w_rope_key, w_key_up, w_value_up, w_out, cache_latent, cache_rope]
-    return pl.pallas_call(
+    rope_in = jnp.swapaxes(cache_rope, 1, 2)
+    held = [w_query, w_latent, w_rope_key.T, w_key_up, w_value_up, w_out, cache_latent, rope_in]
+    mixed, latent_new, rope_new = pl.pallas_call(
         functools.partial(fused_kernel, n, seqs, props, shard_len, width),
         out_shape=(
             jax.ShapeDtypeStruct((seqs, props, out_cols), BF16),
-            jax.ShapeDtypeStruct(cache_latent.shape, BF16),
-            jax.ShapeDtypeStruct(cache_rope.shape, BF16),
+            jax.ShapeDtypeStruct((rows, width), BF16),
+            jax.ShapeDtypeStruct((rows, LANES), BF16),
         ),
         in_specs=[smem] * 3 + [vmem] * 7 + [hbm] * 8,
-        out_specs=(vmem, hbm, hbm),
+        out_specs=(vmem, vmem, vmem),
         scratch_shapes=[pltpu.VMEM(array.shape, array.dtype) for array in held]
         + [
             pltpu.VMEM((rows, model_width), F32),
@@ -555,22 +589,20 @@
             pltpu.VMEM((n // 4, 4 * QK, places), BF16),
             pltpu.VMEM((places, heads_wide), BF16),
             pltpu.VMEM((places, heads_wide), BF16),
-            pltpu.VMEM((n, rows + 8, LANES), F32),
-            pltpu.VMEM((n, rows + 8, LANES), F32),
-            pltpu.VMEM((n, rows + 8, LANES), F32),
+            pltpu.VMEM((n, rows, LANES), F32),
+            pltpu.VMEM((n, rows, LANES), F32),
+            pltpu.VMEM((n, rows, LANES), F32),
             pltpu.VMEM((n, rows, LANES), F32),
             pltpu.VMEM((n, rows, LANES), F32),
             pltpu.VMEM((n, 8, LANES), F32),
             pltpu.VMEM((rows, out_cols), F32),
             pltpu.VMEM((rows, out_cols), F32),
-            pltpu.VMEM((n, 8, LANES), F32),
-            pltpu.VMEM(cache_latent.shape, BF16),
-            pltpu.VMEM(cache_rope.shape, BF16),
+            pltpu.VMEM((n, 1, LANES), F32),
+            pltpu.VMEM((2, rows // 2, width), F32),
             pltpu.SemaphoreType.DMA((len(held),)),
-            pltpu.SemaphoreType.DMA((2,)),
             pltpu.SemaphoreType.DMA((5, n)),
             pltpu.SemaphoreType.DMA((5, n)),
-            pltpu.SemaphoreType.DMA((2,)),
+            pltpu.SemaphoreType.DMA((4,)),
         ],
         compiler_params=pltpu.CompilerParams(
             collective_id=0, has_side_effects=True, vmem_limit_bytes=56 * 1024 * 1024
@@ -579,6 +611,23 @@
         parents, lengths, accepted, tokens, in_gain.reshape(1, -1), latent_gain.reshape(1, -1),
         query_gain.reshape(1, -1), key_gain.reshape(1, -1), out_gain.reshape(1, -1), jnp.asarray(inverse), *held,
     )
+    mixed, new_rope, new_latent = pl.pallas_call(
+        functools.partial(finish_kernel, seqs, props, shard_len, width),
+        out_shape=(
+            jax.ShapeDtypeStruct(mixed.shape, BF16),
+            jax.ShapeDtypeStruct(rope_in.shape, BF16),
+            jax.ShapeDtypeStruct(cache_latent.shape, BF16),
+        ),
+        in_specs=[smem] * 2 + [vmem] * 4 + [hbm],
+        out_specs=(vmem, vmem, hbm),
+        scratch_shapes=[
+            pltpu.VMEM(cache_latent.shape, BF16),
+            pltpu.VMEM(cache_latent.shape, BF16),
+            pltpu.SemaphoreType.DMA((seqs,)),
+            pltpu.SemaphoreType.DMA((seqs,)),
+        ],
+    )(lengths, accepted, mixed, latent_new, rope_new, rope_in, cache_latent)
+    return mixed, new_latent, jnp.swapaxes(new_rope, 1, 2)
 
 
 def step(n, cores, tokens, *others):

time: 48.9 us -> 42.7 us (0.87)
  local copies, waits for them, and re-layouts: 8.94 us -> 0 us
  Pallas kernels: 39 us -> 41.9 us
    unnamed x4 -> x0, local copies, waits for them, and re-layouts: 7.34 us -> none
    pallas_call x0 -> x1, Pallas kernels: none -> 3.89 us  [fused(): pl.pallas_call(functools.partial(finish_kernel, seqs, props, shard_len, w...]
    pallas_call x1 -> x0, local copies, waits for them, and re-layouts: 1.6 us -> none  [fused(): pl.pallas_call(functools.partial(fused_kernel, n, seqs, props, shard_len,...]
    pallas_call x1, Pallas kernels: 39 us -> 38 us  [fused(): pl.pallas_call(functools.partial(fused_kernel, n, seqs, props, shard_len,...]
where the time goes in v2:
time: 42.7 us; the launch traced here: 42.5 us
  Pallas kernels  41.9 us (98%)
  between operations  0.64 us (1%)
    pallas_call x1, Pallas kernels, fused(): pl.pallas_call(functools.partial(fused_kernel, n, seqs, props, shard_len,...  38 us
    pallas_call x1, Pallas kernels, fused(): pl.pallas_call(functools.partial(finish_kernel, seqs, props, shard_len, w...  3.89 us

profile of v2, /device:TPU:0, one launch (start us, length us, event | category | flops | bytes accessed | tf_op | source)
XLA Modules:
  0.0 42.5 jit_solution(11801202847969645966)
XLA Ops:
  0.6 38.0 %shard_map.193 = (bf16[4,4,256]{2,1,0:T(4,128)(2,1)}, bf16[16,1024]{1,0:T(8,128)(2,1)}, bf16[16,128]{1,0:T(8,128)(2,1)}) custom-call(s32[4,4]{1,0:T(4,128)} %parents.1, s32[4]{0:T(128)} %lengths.3, s32[4]{0:T(128)} %accepted.3, bf16[4,4,4096]{2,1,0:T(4,128)(2,1)} %tokens.1, f32[1,4096]{1,0:T(1,128)} %bitcast.11, f32[1,1024]{1,0:T(1,128)} %bitcast.12, ...), custom_call_target="tpu_custom_call" | custom-call | tf_op jit(solution)/shard_map/pallas_call | solution.py:576
  38.6 3.9 %shard_map.194 = (bf16[4,4,256]{2,1,0:T(4,128)(2,1)}, bf16[4,32,128]{2,1,0:T(8,128)(2,1)}, bf16[4,128,1024]{2,1,0:T(8,128)(2,1)}) custom-call(s32[4]{0:T(128)} %lengths.3, s32[4]{0:T(128)} %accepted.3, bf16[4,4,256]{2,1,0:T(4,128)(2,1)} %get-tuple-element.9.mixed, bf16[16,1024]{1,0:T(8,128)(2,1)} %get-tuple-element.10.latent_new, ...), custom_call_target="tpu_custom_call" | custom-call | tf_op jit(solution)/shard_map/pallas_call | solution.py:614

commit v3 on v2

--- a/solution.py
+++ b/solution.py
@@ -247,8 +247,9 @@
         ((wq_h, wq), (wl_h, wl), (cache_h, cache), (rope_h, rope), (wk_h, wk), (wv_h, wv), (wr_h, wr), (wo_h, wo))
     ):
         load = pltpu.make_async_copy(src, dst, load_sem.at[at])
+        loads.append(load)
+    for load in loads[:2]:
         load.start()
-        loads.append(load)
 
     barrier = pltpu.get_barrier_semaphore()
     for off in order:
@@ -266,7 +267,7 @@
             copy_to(phase, off, send.at[lax.rem(me + off, n)], recv.at[off]).start()
 
     def scatter_wait(phase, off, send, recv):
-        copy_to(phase, off, send.at[lax.rem(me + off, n)], recv.at[off]).wait()
+        copy_to(phase, off, send.at[lax.rem(me + off, n)], recv.at[off]).wait_recv()
 
     def gather(phase, table):
         for off in order:
@@ -275,8 +276,6 @@
     def gather_wait(phase, table):
         for off in order:
             copy_to(phase, off, table.at[me], table.at[lax.rem(me - off + n, n)]).wait_recv()
-        for off in order:
-            copy_to(phase, off, table.at[me], table.at[me]).wait_send()
 
     for s in range(seqs):
         x_s[s * props : (s + 1) * props, :] = tokens[s].astype(F32)
@@ -287,6 +286,8 @@
     loads[0].wait()
     q_part = jnp.dot(part, wq[...], preferred_element_type=F32)
     loads[1].wait()
+    for load in loads[2:]:
+        load.start()
     l_part = jnp.dot(part, wl[...], preferred_element_type=F32)
     lane = lane_of((rows, LANES))
     row = row_of((rows, LANES))
@@ -518,29 +519,49 @@
     mixed = (projected * lax.rsqrt(squares / model_width + epsilon) * out_gain[...]).astype(BF16)
     for s in range(seqs):
         mixed_o[s] = mixed[s * props : (s + 1) * props, :]
+    for phase, send in ((0, send_a), (2, send_b)):
+        for off in order:
+            copy_to(phase, off, send.at[lax.rem(me + off, n)], send.at[0]).wait_send()
+    for phase, table in ((1, all_a), (3, all_b), (4, sq_all)):
+        for off in order:
+            copy_to(phase, off, table.at[me], table.at[me]).wait_send()
 
 
 def finish_kernel(
     seqs, props, shard_len, width,
-    lengths, accepted, mixed, latent_new, rope_new, rope_in, cache_h,
-    mixed_o, rope_o, latent_o, cache, out_lat, load_sem, store_sem,
+    lengths, accepted, mixed_h, latent_h, rope_h, rope_in_h, cache_h,
+    mixed_o, rope_o, latent_o, cache, out_lat, mixed, latent_new, rope_new, rope_in, out_rope, load_sem, store_sem,
 ):
     me = lax.axis_index("kv")
     rows = seqs * props
     loads = [pltpu.make_async_copy(cache_h.at[s], cache.at[s], load_sem.at[s]) for s in range(seqs)]
-    for load in loads:
+    small = [
+        pltpu.make_async_copy(src, dst, load_sem.at[seqs + at])
+        for at, (src, dst) in enumerate(
+            ((rope_h, rope_new), (rope_in_h, rope_in), (latent_h, latent_new), (mixed_h, mixed))
+        )
+    ]
+    for load in small + loads:
         load.start()
-    mixed_o[...] = mixed[...]
     slot = lane_of((shard_len, rows))
     chosen = []
+    small[0].wait()
+    small[1].wait()
     for s in range(seqs):
         start = lengths[s] + accepted[s] - me * shard_len
         offset = row_of((shard_len, rows)) - start
         chosen.append(((slot // props == s) & (offset == lax.rem(slot, props))).astype(F32).astype(BF16))
         put_rope = lax.dot_general(rope_new[...], chosen[s], TN, preferred_element_type=F32)[0:ROPE]
         across = lane_of((ROPE, shard_len)) - start
-        rope_o[s] = jnp.where((across >= 0) & (across < props), put_rope, rope_in[s].astype(F32)).astype(BF16)
-    stores = []
+        out_rope[s] = jnp.where((across >= 0) & (across < props), put_rope, rope_in[s].astype(F32)).astype(BF16)
+    small[2].wait()
+    small[3].wait()
+    stores = [
+        pltpu.make_async_copy(out_rope, rope_o, store_sem.at[seqs]),
+        pltpu.make_async_copy(mixed, mixed_o, store_sem.at[seqs + 1]),
+    ]
+    for store in stores:
+        store.start()
     for s in range(seqs):
         put = jnp.dot(chosen[s], latent_new[...], preferred_element_type=F32)
         down = row_of((shard_len, width)) - (lengths[s] + accepted[s] - me * shard_len)
@@ -618,13 +639,18 @@
             jax.ShapeDtypeStruct(rope_in.shape, BF16),
             jax.ShapeDtypeStruct(cache_latent.shape, BF16),
         ),
-        in_specs=[smem] * 2 + [vmem] * 4 + [hbm],
-        out_specs=(vmem, vmem, hbm),
+        in_specs=[smem] * 2 + [hbm] * 5,
+        out_specs=(hbm, hbm, hbm),
         scratch_shapes=[
             pltpu.VMEM(cache_latent.shape, BF16),
             pltpu.VMEM(cache_latent.shape, BF16),
-            pltpu.SemaphoreType.DMA((seqs,)),
-            pltpu.SemaphoreType.DMA((seqs,)),
+            pltpu.VMEM(mixed.shape, BF16),
+            pltpu.VMEM(latent_new.shape, BF16),
+            pltpu.VMEM(rope_new.shape, BF16),
+            pltpu.VMEM(rope_in.shape, BF16),
+            pltpu.VMEM(rope_in.shape, BF16),
+            pltpu.SemaphoreType.DMA((seqs + 4,)),
+            pltpu.SemaphoreType.DMA((seqs + 2,)),
         ],
     )(lengths, accepted, mixed, latent_new, rope_new, rope_in, cache_latent)
     return mixed, new_latent, jnp.swapaxes(new_rope, 1, 2)

time: 42.7 us -> 42.3 us (level)
  Pallas kernels: 41.9 us -> 41.4 us
    pallas_call x1, Pallas kernels: 3.89 us -> 3.43 us  [fused(): pl.pallas_call(functools.partial(finish_kernel, seqs, props, shard_len, w...]
where the time goes in v3:
time: 42.3 us; the launch traced here: 42.1 us
  Pallas kernels  41.4 us (98%)
  between operations  0.64 us (2%)
    pallas_call x1, Pallas kernels, fused(): pl.pallas_call(functools.partial(fused_kernel, n, seqs, props, shard_len,...  38 us
    pallas_call x1, Pallas kernels, fused(): pl.pallas_call(functools.partial(finish_kernel, seqs, props, shard_len, w...  3.43 us

profile of v3, /device:TPU:0, one launch (start us, length us, event | category | flops | bytes accessed | tf_op | source)
XLA Modules:
  0.0 42.1 jit_solution(17718404358985321509)
XLA Ops:
  0.6 38.0 %shard_map.193 = (bf16[4,4,256]{2,1,0:T(4,128)(2,1)}, bf16[16,1024]{1,0:T(8,128)(2,1)}, bf16[16,128]{1,0:T(8,128)(2,1)}) custom-call(s32[4,4]{1,0:T(4,128)} %parents.1, s32[4]{0:T(128)} %lengths.3, s32[4]{0:T(128)} %accepted.3, bf16[4,4,4096]{2,1,0:T(4,128)(2,1)} %tokens.1, f32[1,4096]{1,0:T(1,128)} %bitcast.11, f32[1,1024]{1,0:T(1,128)} %bitcast.12, ...), custom_call_target="tpu_custom_call" | custom-call | tf_op jit(solution)/shard_map/pallas_call | solution.py:597
  38.6 3.4 %shard_map.194 = (bf16[4,4,256]{2,1,0:T(4,128)(2,1)}, bf16[4,32,128]{2,1,0:T(8,128)(2,1)}, bf16[4,128,1024]{2,1,0:T(8,128)(2,1)}) custom-call(s32[4]{0:T(128)} %lengths.3, s32[4]{0:T(128)} %accepted.3, bf16[4,4,256]{2,1,0:T(4,128)(2,1)} %get-tuple-element.9.mixed_h, bf16[16,1024]{1,0:T(8,128)(2,1)} %get-tuple-element.10.latent_h, ...), custom_call_target="tpu_custom_call" | custom-call | tf_op jit(solution)/shard_map/pallas_call | solution.py:635
